TPU v7x, 128 devices: a whole 4x4x4 slice. The times are simulated.
128 devices in a mesh: sp: 16 (over z, x), fs: 4 (over y), tp: 2 (over core).
Axes of the slice: x: 4, y: 4, z: 4, core: 2. Of those that a mesh axis runs over, the one named last changes fastest.
Arguments:
- stream: bfloat16 [4, 16384, 2048], P('fs', 'sp', 'tp'), parts along dimension 0, may hold values from -6 to 6
- w_pool_in: bfloat16 [2048, 1024], P(None, 'tp'), may hold values from -0.125 to 0.125
- w_query: bfloat16 [2048, 1024], P(None, 'tp'), may hold values from -0.125 to 0.125
- w_forget: bfloat16 [2048, 1024], P(None, 'tp'), may hold values from -0.125 to 0.125
- w_value: bfloat16 [2048, 1024], P(None, 'tp'), may hold values from -0.125 to 0.125
- w_outgate: bfloat16 [2048, 1024], P(None, 'tp'), may hold values from -0.125 to 0.125
- pool_mix: bfloat16 [4, 256, 256], P('tp'), may hold values from -0.375 to 0.375
- pool_scale: float32 [1024], P('tp'), may hold values from 0.1 to 1.9
- lower_bound: float32 [1024], P('tp'), may hold values from 0.9 to 1
- extra_decay: float32 [16384, 8], P('sp', 'tp'), may hold values from -0.7 to 0
- rec_gain: float32 [128], replicated, may hold values from 0.1 to 1.9
- w_out_pool: bfloat16 [1024, 2048], P('tp'), may hold values from -0.125 to 0.125
- w_out_rec: bfloat16 [1024, 2048], P('tp'), may hold values from -0.125 to 0.125
- norm_gain: float32 [2048], P('tp'), may hold values from 0.1 to 1.9
- norm_bias: float32 [2048], P('tp'), may hold values from -3 to 3
Outputs:
- layer_out: bfloat16 [4, 16384, 2048], P('fs', 'sp', 'tp'), parts along dimension 0
There are 4 independent parts, one for each index of `fs`. A program takes and returns all parts, laid end to end along the dimension named above; an argument that names none is the same for every part. Nothing has to cross between parts.
All inputs are finite; a program needn't handle non-finite values.
Results may differ from a plain program's by a relative error of at most 0.0085.
Values may be sent and summed in bfloat16 or wider, within the bound.
No kernel may reach another device: no remote copies, remote signals or barrier semaphores. Data moves between devices by JAX's collectives and lax.ppermute only.
A program may use at most 128 MiB of HBM per device.

v0:
```python
import jax
import jax.numpy as jnp
from jax import lax
from jax.sharding import Mesh
from jax.sharding import PartitionSpec as P

D = 2048
DK = 128
WMAX = 16
BLOCK_ROWS = 128
GROUP_CH = 256
SP = ("sp_0", "sp_1")
ALPHA = 2.0**0.25
EPS_RMS = 1e-06
EPS_NORM = 1e-05


def filled_with(x, identity):
    return jax.tree.map(
        lambda a, e: jnp.broadcast_to(jnp.asarray(e, a.dtype), a.shape), x, identity
    )


def gathered_once(x, axis):
    leaves = jax.tree.leaves(x)
    turns = sorted(range(len(leaves)), key=lambda k: -leaves[k].size)
    width = (1, *leaves[turns[0]].shape)[-1]
    lines = [
        jnp.pad(leaves[k].reshape(-1), (0, -leaves[k].size % width)).reshape(-1, width)
        for k in turns
    ]
    both, at, found = (lax.all_gather(jnp.concatenate(lines), axis), 0, {})
    for k, line in zip(turns, lines):
        section = both[:, at : at + len(line)].reshape(len(both), -1)
        found[k] = section[:, : leaves[k].size].reshape(-1, *leaves[k].shape)
        at += len(line)
    numbers = iter(range(len(leaves)))
    return jax.tree.map(lambda _: found[next(numbers)], x)


def entering(x, axes, combine, identity):
    before = start = filled_with(x, identity)
    subtotal = x
    for axis in reversed(axes):
        devices, mine = (lax.axis_size(axis), lax.axis_index(axis))
        pieces = gathered_once(
            jax.tree.map(
                lambda part, kind: part.astype(kind),
                subtotal,
                (jnp.bfloat16, jnp.bfloat16, jnp.bfloat16, jnp.bfloat16),
            ),
            axis,
        )
        inside, subtotal = (start, start)
        for k in range(devices):
            passed = k < mine
            subtotal = combine(
                subtotal, jax.tree.map(lambda part, own: part[k].astype(own.dtype), pieces, x)
            )
            inside = jax.tree.map(lambda new, old: jnp.where(passed, new, old), subtotal, inside)
        before = combine(inside, before)
    return before


def split_up(x, dim, devices):
    before, after = (x.shape[:dim], x.shape[dim + 1 :])
    return jnp.moveaxis(x.reshape(*before, devices, -1, *after), dim, 0)


def summed_on_arrival(x, axis, dim):
    devices = lax.axis_size(axis)
    pieces = lax.all_to_all(split_up(x, dim, devices), axis, 0, 0, tiled=True)
    return jnp.sum(pieces, axis=0)


def total_of_pieces(x, axis):
    pieces = lax.all_gather(x, axis)
    return pieces.sum(axis=0)


def local(
    stream,
    w_pool_in,
    w_query,
    w_forget,
    w_value,
    w_outgate,
    pool_mix,
    pool_scale,
    lower_bound,
    extra_decay,
    rec_gain,
    w_out_pool,
    w_out_rec,
    norm_gain,
    norm_bias,
):
    features = stream[0]
    length = features.shape[0]
    weights = (w_pool_in, w_query, w_forget, w_value, w_outgate)
    column_piece = lax.all_gather(features, "tp", axis=1, tiled=True)
    projected = tuple(
        (jnp.dot(column_piece, weight, preferred_element_type=jnp.float32) for weight in weights)
    )
    pooled, queries, forget_in, value_in, gate_in = [
        projection.astype(jnp.bfloat16) for projection in projected
    ]
    pool_width = pooled.shape[1]
    tail_rows = pooled[length - (WMAX - 1) :]
    channels = lower_bound.shape[0]
    heads_here = channels // DK
    blocks = length // BLOCK_ROWS
    forget = lower_bound + (1.0 - lower_bound) * jax.nn.sigmoid(forget_in.astype(jnp.float32))
    log_keep = (jnp.log(forget).reshape(length, heads_here, DK) + extra_decay[:, :, None]).reshape(
        length, channels
    )
    weight_in = 1.0 - forget
    squashed = jax.nn.silu(queries.astype(jnp.float32))
    row_ids = lax.broadcasted_iota(jnp.int32, (BLOCK_ROWS, BLOCK_ROWS), 0)
    col_ids = lax.broadcasted_iota(jnp.int32, (BLOCK_ROWS, BLOCK_ROWS), 1)
    lower_mask = (row_ids >= col_ids).astype(jnp.float32)
    keep_blocks = log_keep.reshape(blocks, BLOCK_ROWS, channels)
    log_total = jnp.einsum("ts,bsc->btc", lower_mask, keep_blocks)
    log_end = log_total[:, BLOCK_ROWS - 1]
    query_blocks = squashed.reshape(blocks, BLOCK_ROWS, channels)
    input_blocks = weight_in.reshape(blocks, BLOCK_ROWS, channels)
    value_heads = value_in.reshape(blocks, BLOCK_ROWS, heads_here, DK)
    query_up = (query_blocks * jnp.exp(log_total)).reshape(blocks, BLOCK_ROWS, heads_here, DK)
    input_down = (input_blocks * jnp.exp(-log_total)).reshape(blocks, BLOCK_ROWS, heads_here, DK)
    scores = jnp.einsum("bthd,bshd->bhts", query_up, input_down) * lower_mask[None, None]
    inside = jnp.einsum(
        "bhts,bshe->bthe",
        scores.astype(jnp.bfloat16),
        value_heads,
        preferred_element_type=jnp.float32,
    )
    in_weight = (input_blocks * jnp.exp(log_end[:, None] - log_total)).astype(jnp.bfloat16)
    own_terms = jnp.einsum(
        "bshd,bshe->bhde",
        in_weight.reshape(blocks, BLOCK_ROWS, heads_here, DK),
        value_heads,
        preferred_element_type=jnp.float32,
    )

    def block_step(carry, inputs):
        state, offset = carry
        end_blk, term_blk = inputs
        new_state = jnp.exp(end_blk).reshape(heads_here, DK)[:, :, None] * state + term_blk
        return ((new_state, offset + end_blk), (state, offset))

    start_carry = (
        jnp.zeros((heads_here, DK, DK), jnp.float32),
        jnp.zeros((channels,), jnp.float32),
    )
    final_carry, befores = lax.scan(block_step, start_carry, (log_end, own_terms))
    states_before, offsets_before = befores
    carried = jnp.einsum("bthd,bhde->bthe", query_up, states_before)
    local_out = (inside + carried).reshape(length, heads_here, DK)
    query_far = (query_blocks * jnp.exp(offsets_before[:, None] + log_total)).reshape(
        length, heads_here, DK
    )
    local_state = final_carry[0]
    local_keep = jnp.exp(final_carry[1]).reshape(heads_here, DK)
    unit_keep = jnp.ones_like(local_keep)
    empty_state = jnp.zeros_like(local_state)

    def join_all(earlier, later):
        present = later[3] > 0
        return (
            earlier[0] * later[0],
            later[0][:, :, None] * earlier[1] + later[1],
            jnp.where(present, later[2], earlier[2]),
            jnp.maximum(earlier[3], later[3]),
        )

    empty_rows = jnp.zeros(tail_rows.shape, jnp.float32)
    scanned = entering(
        (local_keep, local_state, tail_rows.astype(jnp.float32), jnp.ones((1,), jnp.float32)),
        SP,
        join_all,
        (unit_keep, empty_state, empty_rows, jnp.zeros((1,), jnp.float32)),
    )
    incoming = scanned[1]
    halo_rows = scanned[2].astype(jnp.bfloat16)
    rec_raw = local_out + jnp.einsum("thd,hde->the", query_far, incoming)
    rec_norm = (
        rec_raw
        * lax.rsqrt(jnp.mean(rec_raw * rec_raw, axis=-1, keepdims=True) + EPS_RMS)
        * rec_gain
    )
    gated = rec_norm * jax.nn.silu(gate_in.astype(jnp.float32)).reshape(length, heads_here, DK)
    rec_out = gated.reshape(length, channels).astype(jnp.bfloat16)
    padded = jnp.concatenate([halo_rows, pooled], axis=0).astype(jnp.float32)
    channel_ids = lax.axis_index("tp") * pool_width + lax.iota(jnp.int32, pool_width)
    group_id = channel_ids // GROUP_CH
    window_len = jnp.left_shift(jnp.ones_like(group_id), group_id + 1)
    window_sum = jnp.zeros((length, pool_width), jnp.float32)
    for lag_rows in range(WMAX):
        lagged = padded[WMAX - 1 - lag_rows : WMAX - 1 - lag_rows + length]
        window_sum = window_sum + jnp.where(
            lag_rows < window_len[None, :], lagged, jnp.float32(0.0)
        )
    position = (lax.axis_index(SP) * length + lax.iota(jnp.int32, length) + 1).astype(jnp.float32)
    counts = jnp.minimum(position[:, None], window_len.astype(jnp.float32)[None, :])
    pool_diff = (window_sum / counts - pooled.astype(jnp.float32)).astype(jnp.bfloat16)
    groups_here = pool_mix.shape[0]
    mixed_groups = jnp.einsum(
        "tgc,gcd->tgd",
        pool_diff.reshape(length, groups_here, GROUP_CH),
        pool_mix,
        preferred_element_type=jnp.float32,
    )
    pool_out = (mixed_groups.reshape(length, pool_width) * pool_scale).astype(jnp.bfloat16)
    contract = (((0,), (1,)), ((), ()))
    mixed = summed_on_arrival(
        lax.dot_general(w_out_pool, pool_out, contract, preferred_element_type=jnp.float32)
        + lax.dot_general(w_out_rec, rec_out, contract, preferred_element_type=jnp.float32),
        "tp",
        0,
    ).T
    resid = ALPHA * features.astype(jnp.float32) + mixed
    row_total, squares = (
        total_of_pieces(jnp.sum(resid, axis=1), "tp"),
        total_of_pieces(jnp.sum(resid * resid, axis=1), "tp"),
    )
    row_mean = (row_total / D)[:, None]
    row_var = (squares / D)[:, None] - row_mean * row_mean
    normed = (resid - row_mean) * lax.rsqrt(row_var + EPS_NORM) * norm_gain + norm_bias
    return normed.astype(jnp.bfloat16)[None]


def solution(mesh):
    torus = Mesh(
        mesh.devices.reshape(4, 4, mesh.shape["fs"], mesh.shape["tp"]), ("sp_0", "sp_1", "fs", "tp")
    )
    return jax.shard_map(
        local,
        mesh=torus,
        in_specs=(
            P("fs", SP, "tp"),
            P(None, "tp"),
            P(None, "tp"),
            P(None, "tp"),
            P(None, "tp"),
            P(None, "tp"),
            P("tp", None, None),
            P("tp"),
            P("tp"),
            P(SP, "tp"),
            P(),
            P("tp", None),
            P("tp", None),
            P("tp"),
            P("tp"),
        ),
        out_specs=P("fs", SP, "tp"),
        check_vma=False,
    )
```

profile of v0, /device:TPU:1, one launch (start us, length us, event | category | flops | bytes accessed | tf_op | source)
XLA Modules:
  0.0 219.5 jit_solution(1167471921932692626)
XLA Ops:
  7.7 1.9 copy.110
  15.9 13.1 %all-gather.9.cloned.1.call-done = bf16[1,1024,2048]{2,1,0:T(8,128)(2,1)} async-done(((bf16[1,1024,1024]{2,1,0:T(8,128)(2,1)}), bf16[1,1024,2048]{2,1,0:T(8,128)(2,1)}) %all-gather.9.cloned.1.call-update) | async-done | bytes 4194320 | tf_op jit(solution)/shard_map/all_gather | solution.py:101
  29.0 5.2 %fusion.47 = bf16[1024,512]{1,0:T(8,128)(2,1)S(1)} fusion(bf16[2048,512]{1,0:T(8,128)(2,1)} %param.18, bf16[1,1024,2048]{2,1,0:T(8,128)(2,1)} %all-gather.9.cloned.1.call-done), kind=kOutput, calls=%fused_computation.83 | convolution fusion | flops 2148007936 | bytes 7340032 | tf_op jit(solution)/shard_map/dot_general | solution.py:103
  34.2 1.0 copy-done.6
  35.2 6.2 %fusion.44 = bf16[1024,512]{1,0:T(8,128)(2,1)} fusion(bf16[2048,512]{1,0:T(8,128)(2,1)} %param.21, bf16[1,1024,2048]{2,1,0:T(8,128)(2,1)} %all-gather.9.cloned.1.call-done), kind=kOutput, calls=%fused_computation.82 | convolution fusion | flops 2148007936 | bytes 7340032 | tf_op jit(solution)/shard_map/dot_general | solution.py:103
  41.4 1.3 reshape.465
  42.7 8.2 %broadcast_subtract_fusion = (f32[1024,512]{1,0:T(8,128)}, f32[1024,512]{1,0:T(8,128)}) fusion(bf16[2048,512]{1,0:T(8,128)(2,1)} %param.20, bf16[1,1024,2048]{2,1,0:T(8,128)(2,1)} %all-gather.9.cloned.1.call-done, f32[512]{0:T(512)S(1)} %broadcast_subtract_fusion.1, f32[512]{0:T(512)S(1)} %copy-done.18), kind=kOutput, calls=%fused_computation.92 | convolution fusion | flops 2151677952 | bytes 10489856 | tf_op jit(solution)/shard_map/dot_general | solution.py:103
  51.0 2.9 %copy.78 = f32[8,128,512]{1,2,0:T(8,128)} copy(f32[8,128,512]{2,1,0:T(8,128)} %bitcast.273) | data formatting | bytes 4194304 | tf_op jit(solution)/shard_map/reshape | solution.py:126
  53.9 2.9 %copy.76 = f32[8,128,512]{1,0,2:T(8,128)} copy(f32[8,128,512]{2,1,0:T(8,128)} %bitcast.272) | data formatting | bytes 4194304 | tf_op jit(solution)/shard_map/reshape | solution.py:114
  56.8 2.4 %bitcast_add_fusion.2 = bf16[8,128,512]{1,0,2:T(8,128)(2,1)S(1)} fusion(f32[8,128,512]{1,0,2:T(8,128)} %copy.76, f32[64,8,8,128]{3,2,1,0:T(8,128)} %copy.110), kind=kLoop, calls=%fused_computation.30 | loop fusion | flops 1048576 | bytes 5242880 | tf_op jit(solution)/shard_map/add | solution.py:114
  59.7 1.2 slice_reduce_fusion
  62.0 1.8 fusion.68
  63.8 15.4 %while.17 = (s32[]{:T(128)}, f32[4,128,128]{2,1,0:T(8,128)S(1)}, f32[512]{0:T(512)S(1)}, bf16[8,4,128,128]{3,2,1,0:T(8,128)(2,1)}, f32[8,512]{1,0:T(8,128)S(1)},...) while((s32[]{:T(128)}, f32[4,128,128]{2,1,0:T(8,128)S(1)}, ...), condition=%wide.region_1.2_spmd.clone, body=%wide.region_0.1_spmd.clone.sunk | while | flops 263171 | bytes 1200257 | solution.py:155
  64.5 1.1 bitcast_add_fusion.9
  66.5 1.1 bitcast_add_fusion.9
  68.4 1.1 bitcast_add_fusion.9
  70.3 1.1 bitcast_add_fusion.9
  72.2 1.1 bitcast_add_fusion.9
  74.2 1.1 bitcast_add_fusion.9
  76.1 1.1 bitcast_add_fusion.9
  78.0 1.1 bitcast_add_fusion.9
  79.2 11.5 %all-gather.5 = bf16[4,577,128]{2,1,0:T(8,128)(2,1)S(1)} all-gather(bf16[1,577,128]{2,1,0:T(8,128)(2,1)S(1)} %maximum_bitcast_fusion), channel_id=3, replica_groups=mesh['sp_0'=4,'sp_1'=4,'fs'=4,'tp'=2] {'sp_1'}, dimensions={0}, use_global_device_ids=true | all-gather | bytes 738560 | tf_op jit(solution)/shard_map/all_gather | solution.py:32
  97.9 11.0 %all-gather.6 = bf16[4,577,128]{2,1,0:T(8,128)(2,1)S(1)} all-gather(bf16[1,577,128]{2,1,0:T(8,128)(2,1)S(1)} %maximum_bitcast_fusion.1), channel_id=4, replica_groups=mesh['sp_0'=4,'sp_1'=4,'fs'=4,'tp'=2] {'sp_0'}, dimensions={0}, use_global_device_ids=true | all-gather | bytes 738560 | tf_op jit(solution)/shard_map/all_gather | solution.py:32
  111.4 0.9 slice_convert_fusion.3
  112.4 5.5 %convert_multiply_fusion.1 = f32[1024,512]{1,0:T(8,128)} fusion(bf16[2048,512]{1,0:T(8,128)(2,1)} %param.19, bf16[1,1024,2048]{2,1,0:T(8,128)(2,1)S(1)} %copy-done.38), kind=kOutput, calls=%fused_computation.21 | convolution fusion | flops 2150629376 | bytes 8388608 | tf_op jit(solution)/shard_map/dot_general | solution.py:103
  117.9 2.9 %copy.83 = f32[8,128,512]{1,2,0:T(8,128)} copy(f32[8,128,512]{2,1,0:T(8,128)} %bitcast.274) | data formatting | bytes 4194304 | tf_op jit(solution)/shard_map/reshape | solution.py:125
  120.8 6.8 %convert_multiply_fusion = f32[1024,512]{1,0:T(8,128)} fusion(bf16[2048,512]{1,0:T(8,128)(2,1)} %param.22, bf16[1,1024,2048]{2,1,0:T(8,128)(2,1)} %all-gather.9.cloned.1.call-done), kind=kOutput, calls=%fused_computation.19 | convolution fusion | flops 2150629376 | bytes 8388608 | tf_op jit(solution)/shard_map/dot_general | solution.py:103
  127.6 2.9 %copy.105 = f32[1024,512]{0,1:T(8,128)} copy(f32[1024,512]{1,0:T(8,128)} %convert_multiply_fusion) | data formatting | bytes 4194304 | tf_op jit(solution)/shard_map/reshape | solution.py:191
  130.5 4.1 %exponential_multiply_fusion = (bf16[8,128,512]{1,2,0:T(8,128)(2,1)S(1)}, bf16[8,128,512]{1,2,0:T(8,128)(2,1)S(1)}, bf16[8,128,512]{1,2,0:T(8,128)(2,1)}) fusion(f32[8,128,512]{1,2,0:T(8,128)} %copy.83, f32[8,128,512]{1,2,0:T(8,128)} %copy-done.1, f32[8,512]{1,0:T(8,128)S(1)} %get-tuple-element.48, f32[8,128,512]{1,2,0:T(8,128)} %copy.78), kind=kLoop, calls=%fused_computation.72 | loop fusion | flops 4194304 | bytes 9453568 | tf_op jit(solution)/shard_map/mul | solution.py:159
  134.6 1.6 copy.91
  136.3 2.3 %reshape.477 = bf16[1024,4,128]{0,2,1:T(8,128)(2,1)} reshape(bf16[8,128,512]{1,0,2:T(8,128)(2,1)} %copy.91) | data formatting | bytes 2097152 | tf_op jit(solution)/shard_map/reshape | solution.py:159
  141.8 1.5 select_convert_fusion
  144.1 3.1 %fusion.148 = f32[8,4,128,128]{2,3,1,0:T(8,128)} fusion(bf16[8,4,128,128]{3,2,1,0:T(8,128)(2,1)} %get-tuple-element.47, bf16[8,128,4,128]{1,3,2,0:T(8,128)(2,1)S(1)} %bitcast.263), kind=kOutput, calls=%fused_computation.232 | convolution fusion | flops 134217728 | bytes 4194304 | tf_op jit(solution)/shard_map/bthd,bhde->bthe/dot_general | solution.py:157
  147.1 4.4 %add_bitcast_fusion = f32[8,128,4,128]{3,1,2,0:T(8,128)} fusion(f32[8,4,128,128]{2,3,1,0:T(8,128)} %fusion.148, bf16[8,128,4,128]{1,3,2,0:T(8,128)(2,1)S(1)} %bitcast.264, bf16[8,128,4,128]{1,3,2,0:T(8,128)(2,1)} %bitcast.269, f32[128,128]{1,0:T(8,128)} %fusion.114, bf16[8,128,4,128]{3,2,1,0:T(4,128)(2,1)} %copy-done.3), kind=kOutput, calls=%fused_computation.73 | convolution fusion | flops 270008320 | bytes 7405568 | tf_op jit(solution)/shard_map/bhts,bshe->bthe/dot_general | solution.py:131
  151.5 3.1 %copy.89 = f32[8,128,4,128]{3,1,0,2:T(8,128)} copy(f32[8,128,4,128]{3,1,2,0:T(8,128)} %add_bitcast_fusion) | data formatting | bytes 4194304 | tf_op jit(solution)/shard_map/add | solution.py:158
  154.7 3.0 %copy.94 = f32[1024,4,128]{0,2,1:T(8,128)} copy(f32[1024,4,128]{2,0,1:T(8,128)} %bitcast.266) | data formatting | bytes 4194304 | tf_op jit(solution)/shard_map/reshape | solution.py:158
  157.6 3.3 %multiply_reduce_fusion.1 = (f32[1024,4]{0,1:T(4,128)S(1)}, f32[1024,4,128]{0,2,1:T(8,128)S(1)}) fusion(f32[1024,4,128]{0,2,1:T(8,128)} %copy.94, bf16[1024,4,128]{0,2,1:T(8,128)(2,1)S(1)} %copy-done.8, bf16[4,128,128]{2,1,0:T(8,128)(2,1)} %bitcast.283, bf16[4,128,128]{2,1,0:T(8,128)(2,1)} %bitcast.282, f32[4,128,128]{2,1,0:T(8,128)} %bitcast.278, ...), kind=kOutput, calls=%fused_computation.71 | convolution fusion | flops 137621504 | bytes 6850568 | tf_op jit(solution)/shard_map/thd,hde->the/dot_general | solution.py:185
  161.8 6.2 %fusion.37 = bf16[1024,512]{1,0:T(8,128)(2,1)S(1)} fusion(bf16[1024,512]{1,0:T(8,128)(2,1)S(1)} %copy-done.7, f32[1039,512]{1,0:T(8,128)S(1)} %maximum_convert_fusion, f32[512]{0:T(512)S(1)} %copy-done.14, f32[1024]{0:T(1024)S(1)} %copy-done.13, pred[512]{0:T(512)(128)(4,1)S(1)} %copy-done.34, pred[512]{0:T(512)(128)(4,1)S(1)} %copy-done.35, ...), kind=kLoop, calls=%fused_computation.79 | loop fusion | flops 18874368 | bytes 35665920 | tf_op jit(solution)/shard_map/convert_element_type | solution.py:205
  168.9 2.4 %fusion.147 = f32[1024,2048]{1,0:T(8,128)S(1)} fusion(bf16[1024,512]{0,1:T(8,128)(2,1)S(1)} %fusion.34, bf16[512,2048]{1,0:T(8,128)(2,1)S(1)} %copy-done), kind=kOutput, calls=%fused_computation.231 | convolution fusion | flops 2147483648 | bytes 11534336 | tf_op jit(solution)/shard_map/dot_general | solution.py:216
  171.9 1.0 copy-done.10
  172.9 2.4 %convolution_add_fusion = f32[1024,2048]{1,0:T(8,128)S(1)} fusion(f32[1024,2048]{1,0:T(8,128)S(1)} %fusion.147, bf16[1024,512]{0,1:T(8,128)(2,1)S(1)} %bitcast.268, bf16[512,2048]{1,0:T(8,128)(2,1)S(1)} %copy-done.10), kind=kOutput, calls=%fused_computation.18 | convolution fusion | flops 2149580800 | bytes 19922944 | tf_op jit(solution)/shard_map/dot_general | solution.py:217
  175.4 1.7 copy.126
  177.0 17.0 %all_to_all.5 = f32[2,1024,1024]{1,2,0:T(8,128)} all-to-all(f32[2,1024,1024]{1,2,0:T(8,128)S(1)} %bitcast.262), channel_id=1, replica_groups=mesh['sp_0'=4,'sp_1'=4,'fs'=4,'tp'=2] {'tp'}, dimensions={0} | all-to-all | bytes 16777216 | tf_op jit(solution)/shard_map/all_to_all | solution.py:72
  194.0 6.7 %reduce_sum.55 = f32[1024,1024]{0,1:T(8,128)} reduce(f32[2,1024,1024]{1,2,0:T(8,128)} %all_to_all.5, f32[]{:T(128)} %constant.50.clone.1), dimensions={0}, to_apply=%region_3.4 | reduce | flops 1048576 | bytes 12582916 | tf_op jit(solution)/shard_map/reduce_sum | solution.py:73
  200.7 3.8 %fusion.62 = (f32[1024]{0:T(1024)S(1)}, f32[1024]{0:T(1024)S(1)}) fusion(f32[1024,1024]{0,1:T(8,128)} %reduce_sum.55, bf16[1,1024,1024]{2,1,0:T(8,128)(2,1)} %param.17), kind=kLoop, calls=%fused_computation.86 | loop fusion | flops 6289408 | bytes 6299648 | tf_op jit(solution)/shard_map/reduce_sum | solution.py:223
  204.5 1.8 all-gather.3
  206.4 1.8 all-gather.4
  208.3 4.4 %fusion.16 = bf16[1,1024,1024]{2,1,0:T(8,128)(2,1)} fusion(f32[1024]{0:T(1024)S(1)} %copy-done.16, f32[1024]{0:T(1024)S(1)} %copy-done.17, f32[1024]{0:T(1024)S(1)} %get-tuple-element.119, f32[1024]{0:T(1024)S(1)} %get-tuple-element.118, f32[1024,1024]{0,1:T(8,128)} %reduce_sum.55, bf16[1,1024,1024]{2,1,0:T(8,128)(2,1)} %param.17), kind=kLoop, calls=%fused_computation.29 | loop fusion | flops 8388608 | bytes 8404992 | tf_op jit(solution)/shard_map/broadcast_in_dim | solution.py:229
  (161 shorter events, 23.5 us)
Async XLA Ops:
  6.5 162.3 %copy-start = (bf16[512,2048]{1,0:T(8,128)(2,1)S(1)}, bf16[512,2048]{1,0:T(8,128)(2,1)}, u32[]{:S(2)}) copy-start(bf16[512,2048]{1,0:T(8,128)(2,1)} %param.28) | copy-start | bytes 6291460
  6.5 0.9 copy-start.12
  6.5 22.5 %all-gather.9.cloned.1.call-start = ((), (), s32[]{:S(2)}) async-start(), calls=%async_computation.1 | async-start | bytes 6291456 | tf_op jit(solution)/shard_map/all_gather | solution.py:101
  7.7 8.3 %copy-start.18 = (f32[512]{0:T(512)S(1)}, f32[512]{0:T(512)}, u32[]{:S(2)}) copy-start(f32[512]{0:T(512)} %param.25) | copy-start | bytes 6148
  34.2 1.0 copy-start.6
  42.7 19.2 %copy-start.3 = (bf16[8,128,4,128]{3,2,1,0:T(4,128)(2,1)}, bf16[8,128,4,128]{3,2,1,0:T(4,128)(2,1)S(1)}, u32[]{:S(2)}) copy-start(bf16[8,128,4,128]{3,2,1,0:T(4,128)(2,1)S(1)} %reshape.465) | copy-start | bytes 3145732
  59.2 2.0 copy-start.2
  59.7 2.3 %copy-start.1 = (f32[8,128,512]{1,2,0:T(8,128)}, f32[8,128,512]{1,2,0:T(8,128)S(1)}, u32[]{:S(2)}) copy-start(f32[8,128,512]{1,2,0:T(8,128)S(1)} %fusion.38) | copy-start | bytes 6291460
  63.8 15.4 %copy-start.20 = (bf16[1,128]{1,0:T(2,128)(2,1)S(1)}, bf16[1,128]{1,0:T(2,128)(2,1)}, u32[]{:S(2)}) copy-start(bf16[1,128]{1,0:T(2,128)(2,1)} %constant.36.clone.1) | copy-start | bytes 772
  90.7 20.8 %copy-start.5 = (bf16[4,577,128]{2,1,0:T(8,128)(2,1)}, bf16[4,577,128]{2,1,0:T(8,128)(2,1)S(1)}, u32[]{:S(2)}) copy-start(bf16[4,577,128]{2,1,0:T(8,128)(2,1)S(1)} %all-gather.5) | copy-start | bytes 1772548
  97.5 14.8 %copy-start.38 = (bf16[1,1024,2048]{2,1,0:T(8,128)(2,1)S(1)}, bf16[1,1024,2048]{2,1,0:T(8,128)(2,1)}, u32[]{:S(2)}) copy-start(bf16[1,1024,2048]{2,1,0:T(8,128)(2,1)} %all-gather.9.cloned.1.call-done) | copy-start | bytes 12582916
  108.9 1.8 copy-start.9
  134.6 4.0 %copy-start.15 = (bf16[4,1,128]{2,1,0:T(2,128)(2,1)S(1)}, bf16[4,1,128]{2,1,0:T(2,128)(2,1)}, u32[]{:S(2)}) copy-start(bf16[4,1,128]{2,1,0:T(2,128)(2,1)} %slice.279) | copy-start | bytes 3076
  154.7 3.0 %copy-start.8 = (bf16[1024,4,128]{0,2,1:T(8,128)(2,1)S(1)}, bf16[1024,4,128]{0,2,1:T(8,128)(2,1)}, u32[]{:S(2)}) copy-start(bf16[1024,4,128]{0,2,1:T(8,128)(2,1)} %reshape.477) | copy-start | bytes 3145732
  157.6 3.5 %copy-start.7 = (bf16[1024,512]{1,0:T(8,128)(2,1)S(1)}, bf16[1024,512]{1,0:T(8,128)(2,1)}, u32[]{:S(2)}) copy-start(bf16[1024,512]{1,0:T(8,128)(2,1)} %copy-done.6) | copy-start | bytes 3145732
  161.0 0.7 copy-start.13
  161.0 0.7 copy-start.14
  161.0 0.7 copy-start.22
  161.0 0.7 copy-start.23
  161.0 0.7 copy-start.24
  161.0 0.7 copy-start.25
  161.0 0.6 copy-start.26
  161.0 0.6 copy-start.27
  161.0 0.6 copy-start.28
  161.1 0.6 copy-start.29
  161.1 0.7 copy-start.30
  161.1 0.7 copy-start.31
  161.1 0.7 copy-start.32
  161.1 0.7 copy-start.33
  161.1 0.7 copy-start.34
  161.1 0.7 copy-start.35
  161.1 0.7 copy-start.36
  161.1 0.7 copy-start.37
  161.8 6.2 %copy-start.11 = (bf16[2,256,256]{2,1,0:T(8,128)(2,1)S(1)}, bf16[2,256,256]{2,1,0:T(8,128)(2,1)}, u32[]{:S(2)}) copy-start(bf16[2,256,256]{2,1,0:T(8,128)(2,1)} %param.23) | copy-start | bytes 786436
  168.0 0.7 copy-start.19
  168.8 2.4 %copy-start.4 = (f32[1024,512]{0,1:T(8,128)S(1)}, f32[1024,512]{0,1:T(8,128)}, u32[]{:S(2)}) copy-start(f32[1024,512]{0,1:T(8,128)} %copy.105) | copy-start | bytes 6291460
  168.9 2.4 %copy-start.21 = (f32[128]{0:T(128)S(1)}, f32[128]{0:T(128)}, u32[]{:S(2)}) copy-start(f32[128]{0:T(128)} %param.27) | copy-start | bytes 1540
  171.3 1.6 copy-start.10
  200.7 7.6 %copy-start.16 = (f32[1024]{0:T(1024)S(1)}, f32[1024]{0:T(1024)}, u32[]{:S(2)}) copy-start(f32[1024]{0:T(1024)} %param.31) | copy-start | bytes 12292
  200.7 7.6 %copy-start.17 = (f32[1024]{0:T(1024)S(1)}, f32[1024]{0:T(1024)}, u32[]{:S(2)}) copy-start(f32[1024]{0:T(1024)} %param.30) | copy-start | bytes 12292
Sparse Core Ops, SparseCore 0:
  9.0 19.9 all-gather.8
where the time goes:
time: 221 us; the launch traced here: 220 us
  other arithmetic  55.6 us (25%)
  matrix products  50.2 us (23%)
  blocking collectives  43.1 us (20%)
  local copies, waits for them, and re-layouts  35 us (16%)
  between operations  21.6 us (10%)
  waiting for transfers between devices  13.8 us (6%)
    dot_general x5, matrix products, local(): jnp.dot(column_piece, weight, preferred_element_type=jnp.float32)  31.9 us
    all_gather x2, blocking collectives, gathered_once(): both, at, found = (lax.all_gather(jnp.concatenate(lines), axis), 0, {})  22.4 us
    all_to_all x1, blocking collectives, summed_on_arrival(): pieces = lax.all_to_all(split_up(x, dim, devices), axis, 0, 0, tiled=True)  17 us
    all_gather x1, waiting for transfers between devices, local(): column_piece = lax.all_gather(features, 'tp', axis=1, tiled=True)  13.1 us
    add x8, other arithmetic, block_step(): jnp.exp(end_blk).reshape(heads_here, DK)[:, :, None] * state + term_blk  8.93 us
    reduce_sum x1, other arithmetic, summed_on_arrival(): return jnp.sum(pieces, axis=0)  6.73 us
    convert_element_type x1, other arithmetic, local(): (window_sum / counts - pooled.astype(jnp.float32)).astype(jnp.bfloat16)  6.16 us
    dynamic_update_slice x8, other arithmetic, local(): lax.scan(block_step, start_carry, (log_end, own_terms))  5.44 us
  transfers between devices with their start and end apart: 1, of which 1 were waited for; matrix products, arithmetic and copies ran while one was open for 4% of the time, Pallas kernels for 0%

commit v1 on v0

--- a/solution.py
+++ b/solution.py
@@ -98,7 +98,9 @@
     features = stream[0]
     length = features.shape[0]
     weights = (w_pool_in, w_query, w_forget, w_value, w_outgate)
-    column_piece = lax.all_gather(features, "tp", axis=1, tiled=True)
+    arr_out = lax.axis_size("tp")
+    aux = jnp.concatenate([features] * arr_out, 1)
+    column_piece = lax.all_to_all(aux, "tp", 1, 1, tiled=True)
     projected = tuple(
         (jnp.dot(column_piece, weight, preferred_element_type=jnp.float32) for weight in weights)
     )

time: 221 us -> 212 us (0.959)
  waiting for transfers between devices: 13.8 us -> 0.01 us
  between operations: 21.6 us -> 8.51 us
  starting transfers between devices: 0.01 us -> 7.13 us
  other arithmetic: 55.6 us -> 60.3 us
  local copies, waits for them, and re-layouts: 35 us -> 39.1 us
    all_gather x1 -> x0, waiting for transfers between devices: 13.1 us -> none  [local(): column_piece = lax.all_gather(features, 'tp', axis=1, tiled=True)]
    all_to_all x0 -> x1, starting transfers between devices: none -> 7.13 us  [local(): column_piece = lax.all_to_all(aux, 'tp', 1, 1, tiled=True)]
    concatenate x0 -> x1, other arithmetic: none -> 4.64 us  [local(): aux = jnp.concatenate([features] * arr_out, 1)]
    unnamed x81 -> x80, local copies, waits for them, and re-layouts: 4.8 us -> 8.79 us
  transfers between devices with their start and end apart: 1 -> 1, of which waited for: 1 -> 0; matrix products, arithmetic and copies ran while one was open for 4% -> 4% of each run, Pallas kernels for 0% -> 0%
where the time goes in v1:
time: 212 us; the launch traced here: 211 us
  other arithmetic  60.3 us (28%)
  matrix products  51.7 us (24%)
  blocking collectives  43.9 us (21%)
  local copies, waits for them, and re-layouts  39.1 us (18%)
  between operations  8.51 us (4%)
  starting transfers between devices  7.13 us (3%)
    dot_general x5, matrix products, local(): jnp.dot(column_piece, weight, preferred_element_type=jnp.float32)  33.4 us
    all_gather x2, blocking collectives, gathered_once(): both, at, found = (lax.all_gather(jnp.concatenate(lines), axis), 0, {})  23.1 us
    all_to_all x1, blocking collectives, summed_on_arrival(): pieces = lax.all_to_all(split_up(x, dim, devices), axis, 0, 0, tiled=True)  17.1 us
    add x8, other arithmetic, block_step(): jnp.exp(end_blk).reshape(heads_here, DK)[:, :, None] * state + term_blk  8.93 us
    unnamed x80, local copies, waits for them, and re-layouts  8.79 us
    all_to_all x1, starting transfers between devices, local(): column_piece = lax.all_to_all(aux, 'tp', 1, 1, tiled=True)  7.13 us
    reduce_sum x1, other arithmetic, summed_on_arrival(): return jnp.sum(pieces, axis=0)  6.74 us
    convert_element_type x1, other arithmetic, local(): (window_sum / counts - pooled.astype(jnp.float32)).astype(jnp.bfloat16)  6.13 us
  transfers between devices with their start and end apart: 1, of which 0 were waited for; matrix products, arithmetic and copies ran while one was open for 4% of the time, Pallas kernels for 0%

profile of v1, /device:TPU:1, one launch (start us, length us, event | category | flops | bytes accessed | tf_op | source)
XLA Modules:
  0.0 211.0 jit_solution(13036888244263344273)
XLA Ops:
  0.0 4.1 %copy.78 = bf16[1,1024,1024]{1,2,0:T(8,128)(2,1)} copy(bf16[1,1024,1024]{2,1,0:T(8,128)(2,1)} %param.17) | data formatting | bytes 4194304 | tf_op args[0]
  4.1 4.6 %pad_maximum_fusion = bf16[1024,2,1024]{0,2,1:T(8,128)(2,1)} fusion(bf16[1024,1,1024]{0,2,1:T(8,128)(2,1)} %bitcast.243), kind=kLoop, calls=%fused_computation.5 | loop fusion | flops 2097152 | bytes 6291456 | tf_op jit(solution)/shard_map/concatenate | solution.py:102
  8.7 7.1 %all-to-all-start = ((bf16[1024,2,1024]{0,2,1:T(8,128)(2,1)}), bf16[1024,2,1024]{0,2,1:T(8,128)(2,1)}, u32[]{:S(2)}, u32[]{:S(2)}) async-start(bf16[1024,2,1024]{0,2,1:T(8,128)(2,1)} %pad_maximum_fusion), calls=%async_computation | async-start | bytes 8388608 | tf_op jit(solution)/shard_map/all_to_all | solution.py:103
  22.0 1.8 copy.113
  23.8 5.2 %convolution_convert_fusion.2 = bf16[1024,512]{1,0:T(8,128)(2,1)S(1)} fusion(bf16[1024,2048]{0,1:T(8,128)(2,1)} %bitcast.3, bf16[2048,512]{1,0:T(8,128)(2,1)} %param.18), kind=kOutput, calls=%fused_computation.74 | convolution fusion | flops 2148007936 | bytes 7340032 | tf_op jit(solution)/shard_map/dot_general | solution.py:105
  30.0 6.2 %convolution_convert_fusion.3 = bf16[1024,512]{1,0:T(8,128)(2,1)} fusion(bf16[1024,2048]{0,1:T(8,128)(2,1)} %bitcast.3, bf16[2048,512]{1,0:T(8,128)(2,1)} %param.21), kind=kOutput, calls=%fused_computation.75 | convolution fusion | flops 2148007936 | bytes 7340032 | tf_op jit(solution)/shard_map/dot_general | solution.py:105
  36.2 1.3 reshape.474
  37.6 8.3 %broadcast_subtract_fusion = (f32[1024,512]{1,0:T(8,128)}, f32[1024,512]{1,0:T(8,128)}) fusion(bf16[1024,2048]{0,1:T(8,128)(2,1)} %bitcast.3, bf16[2048,512]{1,0:T(8,128)(2,1)} %param.20, f32[512]{0:T(512)S(1)} %broadcast_subtract_fusion.1, f32[512]{0:T(512)S(1)} %copy-done.18), kind=kOutput, calls=%fused_computation.83 | convolution fusion | flops 2151677952 | bytes 10489856 | tf_op jit(solution)/shard_map/dot_general | solution.py:105
  45.9 3.0 %copy.81 = f32[8,128,512]{1,2,0:T(8,128)} copy(f32[8,128,512]{2,1,0:T(8,128)} %bitcast.252) | data formatting | bytes 4194304 | tf_op jit(solution)/shard_map/reshape | solution.py:128
  48.9 2.9 %copy.79 = f32[8,128,512]{1,0,2:T(8,128)} copy(f32[8,128,512]{2,1,0:T(8,128)} %bitcast.251) | data formatting | bytes 4194304 | tf_op jit(solution)/shard_map/reshape | solution.py:116
  51.7 2.4 %bitcast_add_fusion.2 = bf16[8,128,512]{1,0,2:T(8,128)(2,1)S(1)} fusion(f32[8,128,512]{1,0,2:T(8,128)} %copy.79, f32[64,8,8,128]{3,2,1,0:T(8,128)} %copy.113), kind=kLoop, calls=%fused_computation.21 | loop fusion | flops 1048576 | bytes 5242880 | tf_op jit(solution)/shard_map/add | solution.py:116
  54.6 1.2 slice_reduce_fusion
  56.9 1.8 fusion.37
  58.7 15.4 %while.17 = (s32[]{:T(128)}, f32[4,128,128]{2,1,0:T(8,128)S(1)}, f32[512]{0:T(512)S(1)}, bf16[8,4,128,128]{3,2,1,0:T(8,128)(2,1)}, f32[8,512]{1,0:T(8,128)S(1)},...) while((s32[]{:T(128)}, f32[4,128,128]{2,1,0:T(8,128)S(1)}, ...), condition=%wide.region_1.2_spmd.clone, body=%wide.region_0.1_spmd.clone.sunk | while | flops 263171 | bytes 1200257 | solution.py:157
  59.5 1.1 bitcast_add_fusion.9
  61.4 1.1 bitcast_add_fusion.9
  63.3 1.1 bitcast_add_fusion.9
  65.3 1.1 bitcast_add_fusion.9
  67.2 1.1 bitcast_add_fusion.9
  69.1 1.1 bitcast_add_fusion.9
  71.1 1.1 bitcast_add_fusion.9
  73.0 1.1 bitcast_add_fusion.9
  74.2 11.4 %all-gather.4 = bf16[4,577,128]{2,1,0:T(8,128)(2,1)S(1)} all-gather(bf16[1,577,128]{2,1,0:T(8,128)(2,1)S(1)} %maximum_bitcast_fusion), channel_id=2, replica_groups=mesh['sp_0'=4,'sp_1'=4,'fs'=4,'tp'=2] {'sp_1'}, dimensions={0}, use_global_device_ids=true | all-gather | bytes 738560 | tf_op jit(solution)/shard_map/all_gather | solution.py:32
  93.2 11.7 %all-gather.5 = bf16[4,577,128]{2,1,0:T(8,128)(2,1)S(1)} all-gather(bf16[1,577,128]{2,1,0:T(8,128)(2,1)S(1)} %maximum_bitcast_fusion.1), channel_id=3, replica_groups=mesh['sp_0'=4,'sp_1'=4,'fs'=4,'tp'=2] {'sp_0'}, dimensions={0}, use_global_device_ids=true | all-gather | bytes 738560 | tf_op jit(solution)/shard_map/all_gather | solution.py:32
  109.1 6.9 %convert_multiply_fusion = f32[1024,512]{1,0:T(8,128)} fusion(bf16[1024,2048]{0,1:T(8,128)(2,1)} %bitcast.3, bf16[2048,512]{1,0:T(8,128)(2,1)} %param.22), kind=kOutput, calls=%fused_computation.10 | convolution fusion | flops 2150629376 | bytes 8388608 | tf_op jit(solution)/shard_map/dot_general | solution.py:105
  116.0 2.9 %copy.108 = f32[1024,512]{0,1:T(8,128)} copy(f32[1024,512]{1,0:T(8,128)} %convert_multiply_fusion) | data formatting | bytes 4194304 | tf_op jit(solution)/shard_map/reshape | solution.py:193
  118.9 6.8 %convert_multiply_fusion.1 = f32[1024,512]{1,0:T(8,128)} fusion(bf16[1024,2048]{0,1:T(8,128)(2,1)} %bitcast.3, bf16[2048,512]{1,0:T(8,128)(2,1)} %param.19), kind=kOutput, calls=%fused_computation.12 | convolution fusion | flops 2150629376 | bytes 8388608 | tf_op jit(solution)/shard_map/dot_general | solution.py:105
  125.7 2.9 %copy.86 = f32[8,128,512]{1,2,0:T(8,128)} copy(f32[8,128,512]{2,1,0:T(8,128)} %bitcast.253) | data formatting | bytes 4194304 | tf_op jit(solution)/shard_map/reshape | solution.py:127
  128.7 4.1 %exponential_multiply_fusion = (bf16[8,128,512]{1,2,0:T(8,128)(2,1)S(1)}, bf16[8,128,512]{1,2,0:T(8,128)(2,1)S(1)}, bf16[8,128,512]{1,2,0:T(8,128)(2,1)}) fusion(f32[8,128,512]{1,2,0:T(8,128)} %copy.86, f32[8,128,512]{1,2,0:T(8,128)} %copy-done.1, f32[8,512]{1,0:T(8,128)S(1)} %get-tuple-element.48, f32[8,128,512]{1,2,0:T(8,128)} %copy.81), kind=kLoop, calls=%fused_computation.63 | loop fusion | flops 4194304 | bytes 9453568 | tf_op jit(solution)/shard_map/mul | solution.py:161
  132.8 1.6 copy.94
  134.5 2.3 %reshape.486 = bf16[1024,4,128]{0,2,1:T(8,128)(2,1)} reshape(bf16[8,128,512]{1,0,2:T(8,128)(2,1)} %copy.94) | data formatting | bytes 2097152 | tf_op jit(solution)/shard_map/reshape | solution.py:161
  139.9 1.5 select_convert_fusion
  142.2 3.1 %fusion.117 = f32[8,4,128,128]{2,3,1,0:T(8,128)} fusion(bf16[8,4,128,128]{3,2,1,0:T(8,128)(2,1)} %get-tuple-element.47, bf16[8,128,4,128]{1,3,2,0:T(8,128)(2,1)S(1)} %bitcast.241), kind=kOutput, calls=%fused_computation.223 | convolution fusion | flops 134217728 | bytes 4194304 | tf_op jit(solution)/shard_map/bthd,bhde->bthe/dot_general | solution.py:159
  145.2 4.4 %add_bitcast_fusion = f32[8,128,4,128]{3,1,2,0:T(8,128)} fusion(f32[8,4,128,128]{2,3,1,0:T(8,128)} %fusion.117, bf16[8,128,4,128]{1,3,2,0:T(8,128)(2,1)S(1)} %bitcast.242, bf16[8,128,4,128]{1,3,2,0:T(8,128)(2,1)} %bitcast.248, f32[128,128]{1,0:T(8,128)} %fusion.83, bf16[8,128,4,128]{3,2,1,0:T(4,128)(2,1)} %copy-done.3), kind=kOutput, calls=%fused_computation.64 | convolution fusion | flops 270008320 | bytes 7405568 | tf_op jit(solution)/shard_map/bhts,bshe->bthe/dot_general | solution.py:133
  149.6 3.2 %copy.92 = f32[8,128,4,128]{3,1,0,2:T(8,128)} copy(f32[8,128,4,128]{3,1,2,0:T(8,128)} %add_bitcast_fusion) | data formatting | bytes 4194304 | tf_op jit(solution)/shard_map/add | solution.py:160
  152.8 3.0 %copy.97 = f32[1024,4,128]{0,2,1:T(8,128)} copy(f32[1024,4,128]{2,0,1:T(8,128)} %bitcast.245) | data formatting | bytes 4194304 | tf_op jit(solution)/shard_map/reshape | solution.py:160
  155.8 3.3 %multiply_reduce_fusion.1 = (f32[1024,4]{0,1:T(4,128)S(1)}, f32[1024,4,128]{0,2,1:T(8,128)S(1)}) fusion(f32[1024,4,128]{0,2,1:T(8,128)} %copy.97, bf16[1024,4,128]{0,2,1:T(8,128)(2,1)S(1)} %copy-done.8, bf16[4,128,128]{2,1,0:T(8,128)(2,1)} %bitcast.262, bf16[4,128,128]{2,1,0:T(8,128)(2,1)} %bitcast.261, f32[4,128,128]{2,1,0:T(8,128)} %bitcast.257, ...), kind=kOutput, calls=%fused_computation.62 | convolution fusion | flops 137621504 | bytes 6850568 | tf_op jit(solution)/shard_map/thd,hde->the/dot_general | solution.py:187
  160.0 6.1 %fusion.27 = bf16[1024,512]{1,0:T(8,128)(2,1)S(1)} fusion(bf16[1024,512]{1,0:T(8,128)(2,1)S(1)} %copy-done.7, f32[1039,512]{1,0:T(8,128)S(1)} %maximum_convert_fusion, f32[512]{0:T(512)S(1)} %copy-done.14, f32[1024]{0:T(1024)S(1)} %copy-done.13, pred[512]{0:T(512)(128)(4,1)S(1)} %copy-done.34, pred[512]{0:T(512)(128)(4,1)S(1)} %copy-done.35, ...), kind=kLoop, calls=%fused_computation.70 | loop fusion | flops 18874368 | bytes 35665920 | tf_op jit(solution)/shard_map/convert_element_type | solution.py:207
  167.0 2.4 %fusion.116 = f32[1024,2048]{1,0:T(8,128)S(1)} fusion(bf16[1024,512]{0,1:T(8,128)(2,1)S(1)} %fusion.24, bf16[512,2048]{1,0:T(8,128)(2,1)S(1)} %copy-done), kind=kOutput, calls=%fused_computation.222 | convolution fusion | flops 2147483648 | bytes 11534336 | tf_op jit(solution)/shard_map/dot_general | solution.py:218
  170.1 1.0 copy-done.10
  171.0 2.4 %convolution_add_fusion = f32[1024,2048]{1,0:T(8,128)S(1)} fusion(f32[1024,2048]{1,0:T(8,128)S(1)} %fusion.116, bf16[1024,512]{0,1:T(8,128)(2,1)S(1)} %bitcast.247, bf16[512,2048]{1,0:T(8,128)(2,1)S(1)} %copy-done.10), kind=kOutput, calls=%fused_computation.9 | convolution fusion | flops 2149580800 | bytes 19922944 | tf_op jit(solution)/shard_map/dot_general | solution.py:219
  173.5 1.7 copy.129
  175.2 17.1 %all_to_all.14 = f32[2,1024,1024]{1,2,0:T(8,128)} all-to-all(f32[2,1024,1024]{1,2,0:T(8,128)S(1)} %bitcast.240), channel_id=1, replica_groups=mesh['sp_0'=4,'sp_1'=4,'fs'=4,'tp'=2] {'tp'}, dimensions={0} | all-to-all | bytes 16777216 | tf_op jit(solution)/shard_map/all_to_all | solution.py:72
  192.3 6.7 %reduce_sum.55 = f32[1024,1024]{0,1:T(8,128)} reduce(f32[2,1024,1024]{1,2,0:T(8,128)} %all_to_all.14, f32[]{:T(128)} %constant.50.clone.1), dimensions={0}, to_apply=%region_3.4 | reduce | flops 1048576 | bytes 12582916 | tf_op jit(solution)/shard_map/reduce_sum | solution.py:73
  199.0 3.8 %fusion.31 = (f32[1024]{0:T(1024)S(1)}, f32[1024]{0:T(1024)S(1)}) fusion(f32[1024,1024]{0,1:T(8,128)} %reduce_sum.55, bf16[1,1024,1024]{2,1,0:T(8,128)(2,1)} %param.17), kind=kLoop, calls=%fused_computation.77 | loop fusion | flops 6289408 | bytes 6299648 | tf_op jit(solution)/shard_map/reduce_sum | solution.py:225
  202.8 1.8 all-gather.2
  204.7 1.8 all-gather.3
  206.6 4.4 %fusion.6 = bf16[1,1024,1024]{2,1,0:T(8,128)(2,1)} fusion(f32[1024]{0:T(1024)S(1)} %copy-done.16, f32[1024]{0:T(1024)S(1)} %copy-done.17, f32[1024]{0:T(1024)S(1)} %get-tuple-element.119, f32[1024]{0:T(1024)S(1)} %get-tuple-element.118, f32[1024,1024]{0,1:T(8,128)} %reduce_sum.55, bf16[1,1024,1024]{2,1,0:T(8,128)(2,1)} %param.17), kind=kLoop, calls=%fused_computation.20 | loop fusion | flops 8388608 | bytes 8404992 | tf_op jit(solution)/shard_map/broadcast_in_dim | solution.py:231
  (160 shorter events, 24.8 us)
Async XLA Ops:
  0.0 167.0 %copy-start = (bf16[512,2048]{1,0:T(8,128)(2,1)S(1)}, bf16[512,2048]{1,0:T(8,128)(2,1)}, u32[]{:S(2)}) copy-start(bf16[512,2048]{1,0:T(8,128)(2,1)} %param.28) | copy-start | bytes 6291460
  8.7 13.0 %copy-start.18 = (f32[512]{0:T(512)S(1)}, f32[512]{0:T(512)}, u32[]{:S(2)}) copy-start(f32[512]{0:T(512)} %param.25) | copy-start | bytes 6148
  8.7 13.0 %copy-start.12 = (f32[1024,4]{0,1:T(4,128)S(1)}, f32[1024,4]{0,1:T(4,128)}, u32[]{:S(2)}) copy-start(f32[1024,4]{0,1:T(4,128)} %param.26) | copy-start | bytes 49156
  8.7 15.1 %all-to-all-start = ((bf16[1024,2,1024]{0,2,1:T(8,128)(2,1)}), bf16[1024,2,1024]{0,2,1:T(8,128)(2,1)}, u32[]{:S(2)}, u32[]{:S(2)}) async-start(bf16[1024,2,1024]{0,2,1:T(8,128)(2,1)} %pad_maximum_fusion), calls=%async_computation | async-start | bytes 8388608 | tf_op jit(solution)/shard_map/all_to_all | solution.py:103
  29.0 1.0 copy-start.6
  37.6 19.3 %copy-start.3 = (bf16[8,128,4,128]{3,2,1,0:T(4,128)(2,1)}, bf16[8,128,4,128]{3,2,1,0:T(4,128)(2,1)S(1)}, u32[]{:S(2)}) copy-start(bf16[8,128,4,128]{3,2,1,0:T(4,128)(2,1)S(1)} %reshape.474) | copy-start | bytes 3145732
  54.2 2.0 copy-start.2
  54.6 2.3 %copy-start.1 = (f32[8,128,512]{1,2,0:T(8,128)}, f32[8,128,512]{1,2,0:T(8,128)S(1)}, u32[]{:S(2)}) copy-start(f32[8,128,512]{1,2,0:T(8,128)S(1)} %fusion.28) | copy-start | bytes 6291460
  58.7 15.5 %copy-start.20 = (bf16[1,128]{1,0:T(2,128)(2,1)S(1)}, bf16[1,128]{1,0:T(2,128)(2,1)}, u32[]{:S(2)}) copy-start(bf16[1,128]{1,0:T(2,128)(2,1)} %constant.36.clone.1) | copy-start | bytes 772
  85.6 22.0 %copy-start.5 = (bf16[4,577,128]{2,1,0:T(8,128)(2,1)}, bf16[4,577,128]{2,1,0:T(8,128)(2,1)S(1)}, u32[]{:S(2)}) copy-start(bf16[4,577,128]{2,1,0:T(8,128)(2,1)S(1)} %all-gather.4) | copy-start | bytes 1772548
  105.0 1.8 copy-start.9
  132.8 4.0 %copy-start.15 = (bf16[4,1,128]{2,1,0:T(2,128)(2,1)S(1)}, bf16[4,1,128]{2,1,0:T(2,128)(2,1)}, u32[]{:S(2)}) copy-start(bf16[4,1,128]{2,1,0:T(2,128)(2,1)} %slice.279) | copy-start | bytes 3076
  152.8 3.0 %copy-start.8 = (bf16[1024,4,128]{0,2,1:T(8,128)(2,1)S(1)}, bf16[1024,4,128]{0,2,1:T(8,128)(2,1)}, u32[]{:S(2)}) copy-start(bf16[1024,4,128]{0,2,1:T(8,128)(2,1)} %reshape.486) | copy-start | bytes 3145732
  155.8 3.5 %copy-start.7 = (bf16[1024,512]{1,0:T(8,128)(2,1)S(1)}, bf16[1024,512]{1,0:T(8,128)(2,1)}, u32[]{:S(2)}) copy-start(bf16[1024,512]{1,0:T(8,128)(2,1)} %copy-done.6) | copy-start | bytes 3145732
  159.1 0.7 copy-start.13
  159.1 0.7 copy-start.14
  159.1 0.7 copy-start.22
  159.1 0.7 copy-start.23
  159.1 0.7 copy-start.24
  159.2 0.6 copy-start.25
  159.2 0.7 copy-start.26
  159.2 0.7 copy-start.27
  159.2 0.7 copy-start.28
  159.2 0.7 copy-start.29
  159.2 0.7 copy-start.30
  159.2 0.7 copy-start.31
  159.2 0.6 copy-start.32
  159.2 0.6 copy-start.33
  159.2 0.7 copy-start.34
  159.3 0.7 copy-start.35
  159.3 0.7 copy-start.36
  159.3 0.7 copy-start.37
  160.0 6.2 %copy-start.11 = (bf16[2,256,256]{2,1,0:T(8,128)(2,1)S(1)}, bf16[2,256,256]{2,1,0:T(8,128)(2,1)}, u32[]{:S(2)}) copy-start(bf16[2,256,256]{2,1,0:T(8,128)(2,1)} %param.23) | copy-start | bytes 786436
  166.1 0.7 copy-start.19
  167.0 2.4 %copy-start.4 = (f32[1024,512]{0,1:T(8,128)S(1)}, f32[1024,512]{0,1:T(8,128)}, u32[]{:S(2)}) copy-start(f32[1024,512]{0,1:T(8,128)} %copy.108) | copy-start | bytes 6291460
  167.0 2.4 %copy-start.21 = (f32[128]{0:T(128)S(1)}, f32[128]{0:T(128)}, u32[]{:S(2)}) copy-start(f32[128]{0:T(128)} %param.27) | copy-start | bytes 1540
  169.4 1.6 copy-start.10
  199.0 7.6 %copy-start.16 = (f32[1024]{0:T(1024)S(1)}, f32[1024]{0:T(1024)}, u32[]{:S(2)}) copy-start(f32[1024]{0:T(1024)} %param.31) | copy-start | bytes 12292
  199.0 7.6 %copy-start.17 = (f32[1024]{0:T(1024)S(1)}, f32[1024]{0:T(1024)}, u32[]{:S(2)}) copy-start(f32[1024]{0:T(1024)} %param.30) | copy-start | bytes 12292
